TPU v7x, 32 devices: a whole 2x2x4 slice. The times are simulated.
32 devices in a mesh: ep: 16 (over z, y, x), tp: 2 (over core).
Axes of the slice: x: 2, y: 2, z: 4, core: 2. Of those that a mesh axis runs over, the one named last changes fastest.
Arguments:
- tokens: bfloat16 [512, 2048], P('ep'), may hold values from -6 to 6
- lengths: int32 [512], P('ep'), may hold values from 128 to 1024
- key_cache: bfloat16 [512, 1024, 256], P('ep', None, 'tp'), may hold values from -1000 to 1000
- value_cache: bfloat16 [512, 1024, 256], P('ep', None, 'tp'), may hold values from -6 to 6
- gate_cache: float32 [512, 16, 1024], P('ep', 'tp'), may hold values from -130 to 0, as said below
- mix_gain: float32 [2048], replicated, may hold values from 0.1 to 1.9
- query_weight: bfloat16 [2048, 1024], P(None, 'tp'), may hold values from -0.125 to 0.125
- key_weight: bfloat16 [2048, 256], P(None, 'tp'), may hold values from -0.125 to 0.125
- value_weight: bfloat16 [2048, 256], P(None, 'tp'), may hold values from -0.125 to 0.125
- forget_weight: bfloat16 [2048, 16], P(None, 'tp'), may hold values from -0.125 to 0.125
- out_weight: bfloat16 [1024, 2048], P('tp'), may hold values from -0.1875 to 0.1875
- expert_gain: float32 [2048], replicated, may hold values from 0.1 to 1.9
- routes: int32 [512, 2], P('ep'), may hold values from 0 to 7, all different within a row; in each aligned block of 32 rows (0 to 31, 32 to 63, ...) at most 12 rows name the same one
- route_weights: float32 [512, 2], P('ep'), may hold values from 0.2 to 1
- expert_gate: bfloat16 [2048, 65536], P(None, ('ep', 'tp')), may hold values from -0.125 to 0.125
- expert_up: bfloat16 [2048, 65536], P(None, ('ep', 'tp')), may hold values from -0.125 to 0.125
- expert_down: bfloat16 [65536, 2048], P(('ep', 'tp')), may hold values from -0.0625 to 0.0625
Outputs:
- layer_out: bfloat16 [512, 2048], P('ep')
Inputs may be any that keep to these rules, and one draw needn't show every extreme that they name: `routes`: within the rows of one index of ep, no expert is named more than 12 times, and in every draw some expert is named exactly 12 times in some such rows; the 2 experts of a row differ. `gate_cache`: for each sequence and head the values never rise along the cache positions.
All inputs are finite; a program needn't handle non-finite values.
Results may differ from a plain program's by a relative error of at most 0.013.
Values may be sent and summed in bfloat16 or wider, within the bound.
A program may use at most 128 MiB of HBM per device.

v0:
```python
import jax
import jax.numpy as jnp
from jax import lax
from jax.sharding import PartitionSpec as P

HD = 64
EXPERTS = 8
CAP = 12
eps = 1e-06


def normed(values, gain):
    floats = values.astype(jnp.float32)
    return floats * lax.rsqrt(jnp.mean(floats * floats, axis=-1, keepdims=True) + eps) * gain


def attend(queries, key_new, value_new, log_gate, key_rows, value_rows, cumulative, length):
    seq_count, head_count, head_size = queries.shape
    kv_count = key_new.shape[1]
    group_size = head_count // kv_count
    cache_locations = key_rows.shape[1]
    factor = head_size ** (-0.5)
    grouped = queries.reshape(seq_count, kv_count, group_size, head_size)
    key_split = key_rows.reshape(seq_count, cache_locations, kv_count, head_size)
    value_split = value_rows.reshape(seq_count, cache_locations, kv_count, head_size)
    scores = (
        jnp.einsum(
            "skgd,spkd->skgp", grouped, key_split, preferred_element_type=jnp.float32
        ).reshape(seq_count, head_count, cache_locations)
        * factor
    )
    positions = jnp.arange(cache_locations, dtype=jnp.int32)
    latest = jnp.sum(
        jnp.where(positions[None, None, :] == (length - 1)[:, None, None], cumulative, 0.0), axis=-1
    )
    scores = scores + (latest + log_gate)[..., None] - cumulative
    valid = positions[None, None, :] < length[:, None, None]
    scores = jnp.where(valid, scores, -jnp.inf)
    own_score = (
        jnp.einsum("skgd,skd->skg", grouped, key_new, preferred_element_type=jnp.float32).reshape(
            seq_count, head_count
        )
        * factor
    )
    highest = jnp.maximum(jnp.max(scores, axis=-1), own_score)
    raised = jnp.exp(scores - highest[..., None])
    own_raised = jnp.exp(own_score - highest)
    denominator = jnp.sum(raised, axis=-1) + own_raised
    weights = (raised / denominator[..., None]).astype(jnp.bfloat16)
    own_weight = (own_raised / denominator).astype(jnp.bfloat16)
    mixed = jnp.einsum(
        "skgp,spkd->skgd",
        weights.reshape(seq_count, kv_count, group_size, cache_locations),
        value_split,
        preferred_element_type=jnp.float32,
    )
    mixed = (
        mixed
        + own_weight.reshape(seq_count, kv_count, group_size)[..., None].astype(jnp.float32)
        * value_new.astype(jnp.float32)[:, :, None, :]
    )
    return mixed.reshape(seq_count, head_count * head_size).astype(jnp.bfloat16)


def expert_work(rows_in, expert_gate, expert_up, expert_down):
    leading = rows_in.shape[:-1]
    flat_rows = rows_in.reshape(-1, rows_in.shape[-1])
    gate_out = jnp.dot(flat_rows, expert_gate, preferred_element_type=jnp.float32)
    up_out = jnp.dot(flat_rows, expert_up, preferred_element_type=jnp.float32)
    hidden = (jax.nn.silu(gate_out) * up_out).astype(jnp.bfloat16)
    return jnp.dot(hidden, expert_down, preferred_element_type=jnp.float32).reshape(
        leading + (expert_down.shape[1],)
    )


def combine(returned, target, route_weights):
    capacity = returned.shape[1]
    columns = returned.shape[2]
    blocks = jnp.sum(
        returned.reshape(EXPERTS, -1, capacity, columns).astype(jnp.float32), axis=1
    ).reshape(EXPERTS * capacity, columns)
    picked = jnp.take(blocks, target, axis=0).reshape(route_weights.shape + (columns,))
    return jnp.sum(picked * route_weights[..., None], axis=1)


def on_device(
    tokens,
    lengths,
    key_cache,
    value_cache,
    gate_cache,
    mix_gain,
    query_weight,
    key_weight,
    value_weight,
    forget_weight,
    out_weight,
    expert_gain,
    routes,
    route_weights,
    expert_gate,
    expert_up,
    expert_down,
):
    seq_count = tokens.shape[0]
    width = tokens.shape[1]
    normal_in = normed(tokens, mix_gain).astype(jnp.bfloat16)
    queries = (
        jnp.dot(normal_in, query_weight, preferred_element_type=jnp.float32)
        .astype(jnp.bfloat16)
        .reshape(seq_count, -1, HD)
    )
    key_new = (
        jnp.dot(normal_in, key_weight, preferred_element_type=jnp.float32)
        .astype(jnp.bfloat16)
        .reshape(seq_count, -1, HD)
    )
    value_new = (
        jnp.dot(normal_in, value_weight, preferred_element_type=jnp.float32)
        .astype(jnp.bfloat16)
        .reshape(seq_count, -1, HD)
    )
    log_gate = jax.nn.log_sigmoid(
        jnp.dot(normal_in, forget_weight, preferred_element_type=jnp.float32)
    )
    mixed = attend(
        queries, key_new, value_new, log_gate, key_cache, value_cache, gate_cache, lengths
    )
    partial_out = jnp.dot(mixed, out_weight, preferred_element_type=jnp.float32).astype(
        jnp.bfloat16
    )
    residual = (
        tokens.astype(jnp.float32) + lax.psum(partial_out, "tp").astype(jnp.float32)
    ).astype(jnp.bfloat16)
    expert_in = normed(residual, expert_gain).astype(jnp.bfloat16)
    top_count = routes.shape[1]
    flat_routes = routes.reshape(-1)
    one_hot = (flat_routes[:, None] == jnp.arange(EXPERTS, dtype=jnp.int32)[None, :]).astype(
        jnp.int32
    )
    slot_index = jnp.sum((jnp.cumsum(one_hot, axis=0) - 1) * one_hot, axis=1)
    target = flat_routes * CAP + slot_index
    dispatch = (jnp.arange(EXPERTS * CAP, dtype=jnp.int32)[:, None] == target[None, :]).astype(
        jnp.bfloat16
    )
    repeated = jnp.repeat(expert_in, top_count, axis=0)
    outgoing = jnp.dot(dispatch, repeated, preferred_element_type=jnp.float32).astype(jnp.bfloat16)
    pieces = lax.axis_size("ep") // EXPERTS
    outgoing = jnp.broadcast_to(
        outgoing.reshape(EXPERTS, 1, CAP, width), (EXPERTS, pieces, CAP, width)
    ).reshape(EXPERTS * pieces, CAP, width)
    half_width = width // lax.axis_size("tp")
    start = lax.axis_index("tp") * half_width
    outgoing_half = lax.dynamic_slice_in_dim(outgoing, start, half_width, 2)
    full_rows = lax.all_gather(
        lax.all_to_all(outgoing_half, "ep", split_axis=0, concat_axis=0, tiled=True),
        "tp",
        axis=2,
        tiled=True,
    )
    partial_rows = expert_work(full_rows, expert_gate, expert_up, expert_down).astype(jnp.bfloat16)
    share = (
        lax.psum_scatter(partial_rows, "tp", scatter_dimension=2, tiled=True)
        .astype(jnp.float32)
        .astype(jnp.bfloat16)
    )
    returned = lax.all_to_all(share, "ep", split_axis=0, concat_axis=0, tiled=True)
    mixture = combine(returned, target, route_weights)
    own_half = lax.dynamic_slice_in_dim(residual, start, half_width, 1).astype(jnp.float32)
    return lax.all_gather((own_half + mixture).astype(jnp.bfloat16), "tp", axis=1, tiled=True)


def solution(mesh):
    return jax.shard_map(
        on_device,
        mesh=mesh,
        in_specs=(
            P("ep", None),
            P("ep"),
            P("ep", None, "tp"),
            P("ep", None, "tp"),
            P("ep", "tp", None),
            P(),
            P(None, "tp"),
            P(None, "tp"),
            P(None, "tp"),
            P(None, "tp"),
            P("tp", None),
            P(),
            P("ep", None),
            P("ep", None),
            P(None, ("ep", "tp")),
            P(None, ("ep", "tp")),
            P(("ep", "tp"), None),
        ),
        out_specs=P("ep", None),
        check_vma=False,
    )
```

profile of v0, /device:TPU:0, one launch (start us, length us, event | category | flops | bytes accessed | tf_op | source)
XLA Modules:
  0.0 167.7 jit_solution(255999665573253015)
XLA Ops:
  6.5 0.8 broadcast_add_fusion
  7.3 0.7 iota_compare_fusion.1
  8.1 1.0 fusion.7
  9.1 2.2 %convolution_convert_fusion.3 = bf16[32,512]{1,0:T(8,128)(2,1)S(1)} fusion(bf16[2048,512]{1,0:T(8,128)(2,1)} %param.23, bf16[32,2048]{1,0:T(8,128)(2,1)} %param.17, f32[2048]{0:T(1024)} %param.22, f32[32]{0:T(128)S(1)} %add_rsqrt_fusion.1), kind=kOutput, calls=%fused_computation.9 | convolution fusion | flops 67387392 | bytes 2269312 | tf_op jit(solution)/shard_map/dot_general | solution.py:109
  11.3 0.1 reshape_reshape.3
  11.5 11.9 %copy.45 = bf16[32,1024,128]{1,2,0:T(8,128)(2,1)} copy(bf16[32,1024,128]{2,1,0:T(8,128)(2,1)} %param.19) | data formatting | bytes 16777216 | tf_op args[2]
  23.4 4.6 %convolution_multiply_fusion.1 = f32[32,2,4,1024]{3,2,1,0:T(4,128)S(1)} fusion(bf16[32,2,4,64]{3,2,1,0:T(4,128)(2,1)S(1)} %reshape_reshape.3, bf16[32,1024,2,64]{1,3,2,0:T(8,128)(2,1)} %bitcast.37), kind=kOutput, calls=%fused_computation.6 | convolution fusion | flops 33816576 | bytes 9469952 | tf_op jit(solution)/shard_map/skgd,spkd->skgp/dot_general | solution.py:27
  28.0 1.4 mul.132
  29.4 0.1 iota_compare_fusion
  29.5 1.5 select_reduce_fusion
  31.0 0.2 fusion.15
  31.2 0.1 copy.47
  31.3 1.9 %fusion.25 = (f32[32,8]{1,0:T(8,128)S(1)}, f32[32,8,1024]{2,1,0:T(8,128)S(1)}) fusion(f32[32,8,1024]{2,1,0:T(8,128)} %param.21, f32[32,8,1024]{2,1,0:T(8,128)} %mul.132, f32[32,8]{1,0:T(8,128)S(1)} %copy.47, pred[32,1024]{1,0:T(8,128)(4,1)S(1)} %iota_compare_fusion.1), kind=kLoop, calls=%fused_computation.64 | loop fusion | flops 1048320 | bytes 3180544 | tf_op jit(solution)/shard_map/reduce_max | solution.py:45
  33.3 1.3 convolution_convert_fusion.5
  34.6 0.1 reshape.208
  34.7 0.2 fusion.26
  34.9 0.1 copy.62
  35.0 0.1 copy.49
  35.1 0.3 fusion.3
  35.5 0.1 copy.51
  35.5 1.1 divide_convert_fusion
  36.6 1.2 reshape.188
  37.9 0.1 copy.55
  38.0 1.3 fusion.2
  39.3 0.1 reshape.195
  39.4 11.9 %copy.52 = bf16[32,1024,128]{1,2,0:T(8,128)(2,1)} copy(bf16[32,1024,128]{2,1,0:T(8,128)(2,1)} %param.20) | data formatting | bytes 16777216 | tf_op args[3]
  51.3 5.7 %fusion.1 = bf16[32,2,4,64]{3,2,1,0:T(4,128)(2,1)S(1)} fusion(bf16[32,2,4,1024]{3,2,1,0:T(4,128)(2,1)S(1)} %reshape.188, bf16[32,1024,2,64]{1,3,2,0:T(8,128)(2,1)} %bitcast.38, f32[32,2,64]{2,1,0:T(2,128)S(1)} %reshape.195, f32[32,2,4]{2,1,0:T(2,128)S(1)} %copy.55), kind=kOutput, calls=%fused_computation.8 | convolution fusion | flops 33603584 | bytes 8963072 | tf_op jit(solution)/shard_map/skgp,spkd->skgd/dot_general | solution.py:51
  57.0 0.1 convert_element_type.99
  57.1 1.1 convolution_convert_fusion.2
  58.4 0.1 copy.56
  58.5 0.1 reshape.190
  58.6 0.1 reduce_window_sum.11
  58.7 0.2 select_reduce_fusion.1
  58.9 20.2 %all-reduce.2.cloned.1.call-done = bf16[32,2048]{1,0:T(8,128)(2,1)} async-done(((bf16[32,2048]{1,0:T(8,128)(2,1)}), bf16[32,2048]{1,0:T(8,128)(2,1)}) %all-reduce.2.cloned.1.call-update) | async-done | bytes 131088 | tf_op jit(solution)/shard_map/psum | solution.py:133
  79.1 1.1 fusion.4
  80.2 0.1 fusion.6
  80.3 0.5 copy-done.3
  80.8 0.1 broadcast_in_dim.61
  81.0 0.1 reshape.191
  81.1 0.2 convolution_convert_fusion.1
  81.3 0.1 broadcast_in_dim.62
  81.4 0.1 broadcast_in_dim.63
  81.6 22.1 %all_to_all.10 = bf16[16,12,1024]{2,1,0:T(8,128)(2,1)S(1)} all-to-all(bf16[16,12,1024]{2,1,0:T(8,128)(2,1)S(1)} %constant_dynamic-slice_fusion), channel_id=1, replica_groups=mesh['ep'=16,'tp'=2] {'ep'}, dimensions={0} | all-to-all | bytes 786432 | tf_op jit(solution)/shard_map/all_to_all | solution.py:156
  103.7 2.7 %all_gather.6 = bf16[16,12,2048]{2,1,0:T(8,128)(2,1)S(1)} all-gather(bf16[16,12,1024]{2,1,0:T(8,128)(2,1)S(1)} %all_to_all.10), channel_id=1, replica_groups=mesh['ep'=16,'tp'=2] {'tp'}, dimensions={2}, use_global_device_ids=true | all-gather | bytes 1179648 | tf_op jit(solution)/shard_map/all_gather | solution.py:155
  106.5 0.2 reshape.193
  106.6 6.3 %fusion.27 = f32[192,2048]{1,0:T(8,128)} fusion(bf16[192,2048]{1,0:T(8,128)(2,1)S(1)} %reshape.193, bf16[2048,2048]{1,0:T(8,128)(2,1)} %param.31), kind=kOutput, calls=%fused_computation.66 | convolution fusion | flops 1610612736 | bytes 10747904 | tf_op jit(solution)/shard_map/dot_general | solution.py:68
  113.0 10.9 %convolution_convert_fusion = bf16[192,2048]{1,0:T(8,128)(2,1)} fusion(bf16[2048,2048]{1,0:T(8,128)(2,1)} %param.33, bf16[192,2048]{1,0:T(8,128)(2,1)S(1)} %reshape.193, bf16[2048,2048]{1,0:T(8,128)(2,1)} %param.32, f32[192,2048]{1,0:T(8,128)} %fusion.27), kind=kOutput, calls=%fused_computation.2 | convolution fusion | flops 3223977984 | bytes 19922944 | tf_op jit(solution)/shard_map/dot_general | solution.py:71
  123.8 2.1 %convert_element_type.110 = bf16[16,12,2048]{2,1,0:T(8,128)(2,1)} reshape(bf16[192,2048]{1,0:T(8,128)(2,1)} %convolution_convert_fusion) | data formatting | bytes 1572864 | tf_op jit(solution)/shard_map/convert_element_type | solution.py:161
  126.0 0.1 reduce_sum.74
  126.1 6.8 %reduce-scatter.2.cloned.1.call-done = bf16[16,12,1024]{2,1,0:T(8,128)(2,1)} async-done(((bf16[16,12,2048]{2,1,0:T(8,128)(2,1)}), bf16[16,12,1024]{2,1,0:T(8,128)(2,1)}) %reduce-scatter.2.cloned.1.call-update) | async-done | bytes 393232 | tf_op jit(solution)/shard_map/reduce_scatter | solution.py:163
  132.9 6.8 %all-to-all-start.1 = ((bf16[16,12,1024]{2,1,0:T(8,128)(2,1)}), bf16[16,12,1024]{2,1,0:T(8,128)(2,1)S(1)}, u32[]{:S(2)}, u32[]{:S(2)}) async-start(bf16[16,12,1024]{2,1,0:T(8,128)(2,1)} %reduce-scatter.2.cloned.1.call-done), calls=%async_computation.2 | async-start | bytes 1048576 | tf_op jit(solution)/shard_map/all_to_all | solution.py:167
  139.7 0.1 copy.59
  139.8 0.1 mul.152
  140.0 0.7 copy.58
  140.7 0.1 copy.60
  140.7 0.6 pad_clamp_fusion
  141.3 13.8 %all-to-all-done.1 = bf16[16,12,1024]{2,1,0:T(8,128)(2,1)S(1)} async-done(((bf16[16,12,1024]{2,1,0:T(8,128)(2,1)}), bf16[16,12,1024]{2,1,0:T(8,128)(2,1)S(1)}, u32[]{:S(2)}, u32[]{:S(2)}) %all-to-all-start.1) | async-done | bytes 393248 | tf_op jit(solution)/shard_map/all_to_all | solution.py:167
  155.1 0.1 convert_reduce_fusion
  155.3 0.8 gather_fusion
  156.1 0.1 gather.7
  156.3 1.2 multiply_reduce_fusion
  157.4 0.9 add_convert_fusion
  158.3 1.9 %all_gather.7 = bf16[32,2048]{1,0:T(8,128)(2,1)S(1)} all-gather(bf16[32,1024]{1,0:T(8,128)(2,1)S(1)} %add_convert_fusion), channel_id=1, replica_groups=mesh['ep'=16,'tp'=2] {'tp'}, dimensions={1}, use_global_device_ids=true | all-gather | bytes 196608 | tf_op jit(solution)/shard_map/all_gather | solution.py:170
  160.2 0.7 copy.65
  (38 shorter events, 0.6 us)
Async XLA Ops:
  6.5 50.6 %copy-start = (bf16[512,2048]{1,0:T(8,128)(2,1)S(1)}, bf16[512,2048]{1,0:T(8,128)(2,1)}, u32[]{:S(2)}) copy-start(bf16[512,2048]{1,0:T(8,128)(2,1)} %param.27) | copy-start | bytes 6291460
  6.5 72.6 %all-reduce.2.cloned.1.call-start = ((), (), s32[]{:S(2)}) async-start(), calls=%async_computation.3 | async-start | bytes 262144 | tf_op jit(solution)/shard_map/psum | solution.py:133
  23.4 7.6 %copy-start.2 = (bf16[32,2048]{1,0:T(8,128)(2,1)S(1)}, bf16[32,2048]{1,0:T(8,128)(2,1)}, u32[]{:S(2)}) copy-start(bf16[32,2048]{1,0:T(8,128)(2,1)} %param.17) | copy-start | bytes 393220
  23.4 7.6 %copy-start.4 = (f32[2048]{0:T(1024)S(1)}, f32[2048]{0:T(1024)}, u32[]{:S(2)}) copy-start(f32[2048]{0:T(1024)} %param.22) | copy-start | bytes 24580
  23.4 7.6 %copy-start.8 = (bf16[2048,8]{0,1:T(8,128)(2,1)S(1)}, bf16[2048,8]{0,1:T(8,128)(2,1)}, u32[]{:S(2)}) copy-start(bf16[2048,8]{0,1:T(8,128)(2,1)} %param.26) | copy-start | bytes 98308
  51.3 7.0 %copy-start.5 = (s32[32,2]{0,1:T(2,128)S(1)}, s32[32,2]{0,1:T(2,128)}, u32[]{:S(2)}) copy-start(s32[32,2]{0,1:T(2,128)} %param.29) | copy-start | bytes 772
  51.3 28.9 %copy-start.6 = (f32[2048]{0:T(1024)S(1)}, f32[2048]{0:T(1024)}, u32[]{:S(2)}) copy-start(f32[2048]{0:T(1024)} %param.28) | copy-start | bytes 24580
  58.3 74.6 %reduce-scatter.2.cloned.1.call-start = ((), (), s32[]{:S(2)}) async-start(), calls=%async_computation.4 | async-start | bytes 1572864 | tf_op jit(solution)/shard_map/reduce_scatter | solution.py:163
  80.2 0.7 copy-start.3
  113.0 27.7 %copy-start.7 = (f32[32,2]{0,1:T(2,128)S(1)}, f32[32,2]{0,1:T(2,128)}, u32[]{:S(2)}) copy-start(f32[32,2]{0,1:T(2,128)} %param.30) | copy-start | bytes 772
  113.0 47.9 %copy-start.1 = (bf16[512,2048]{1,0:T(8,128)(2,1)S(1)}, bf16[512,2048]{1,0:T(8,128)(2,1)}, u32[]{:S(2)}) copy-start(bf16[512,2048]{1,0:T(8,128)(2,1)} %param.27) | copy-start | bytes 6291460
  132.9 22.3 %all-to-all-start.1 = ((bf16[16,12,1024]{2,1,0:T(8,128)(2,1)}), bf16[16,12,1024]{2,1,0:T(8,128)(2,1)S(1)}, u32[]{:S(2)}, u32[]{:S(2)}) async-start(bf16[16,12,1024]{2,1,0:T(8,128)(2,1)} %reduce-scatter.2.cloned.1.call-done), calls=%async_computation.2 | async-start | bytes 1048576 | tf_op jit(solution)/shard_map/all_to_all | solution.py:167
Sparse Core Ops, SparseCore 0:
  58.4 20.6 all-reduce.1
  126.1 6.7 reduce-scatter.1
where the time goes:
time: 169 us; the launch traced here: 168 us
  waiting for transfers between devices  40.8 us (24%)
  matrix products  34.1 us (20%)
  local copies, waits for them, and re-layouts  33.9 us (20%)
  blocking collectives  26.7 us (16%)
  between operations  13.7 us (8%)
  other arithmetic  11.7 us (7%)
  starting transfers between devices  6.82 us (4%)
    unnamed x23, local copies, waits for them, and re-layouts  25.3 us
    all_to_all x1, blocking collectives, on_device(): lax.all_to_all(outgoing_half, 'ep', split_axis=0, concat_axis=0, tiled=True)  22.1 us
    psum x1, waiting for transfers between devices, on_device(): lax.psum(partial_out, 'tp').astype(jnp.float32)  20.2 us
    all_to_all x1, waiting for transfers between devices, on_device(): lax.all_to_all(share, 'ep', split_axis=0, concat_axis=0, tiled=True)  13.8 us
    dot_general x1, matrix products, expert_work(): jnp.dot(hidden, expert_down, preferred_element_type=jnp.float32)  10.9 us
    all_to_all x1, starting transfers between devices, on_device(): lax.all_to_all(share, 'ep', split_axis=0, concat_axis=0, tiled=True)  6.78 us
    reduce_scatter x1, waiting for transfers between devices, on_device(): lax.psum_scatter(partial_rows, 'tp', scatter_dimension=2, tiled=True)  6.77 us
    dot_general x1, matrix products, expert_work(): jnp.dot(flat_rows, expert_gate, preferred_element_type=jnp.float32)  6.34 us
  transfers between devices with their start and end apart: 3, of which 3 were waited for; matrix products, arithmetic and copies ran while one was open for 1% of the time, Pallas kernels for 0%

commit v1 on v0

--- a/solution.py
+++ b/solution.py
@@ -129,9 +129,10 @@
     partial_out = jnp.dot(mixed, out_weight, preferred_element_type=jnp.float32).astype(
         jnp.bfloat16
     )
-    residual = (
-        tokens.astype(jnp.float32) + lax.psum(partial_out, "tp").astype(jnp.float32)
-    ).astype(jnp.bfloat16)
+    end_marks = lambda own_rows: jnp.sum(jax.lax.all_gather(own_rows, axis_name="tp"), axis=0)
+    residual = (tokens.astype(jnp.float32) + end_marks(partial_out).astype(jnp.float32)).astype(
+        jnp.bfloat16
+    )
     expert_in = normed(residual, expert_gain).astype(jnp.bfloat16)
     top_count = routes.shape[1]
     flat_routes = routes.reshape(-1)

time: 169 us -> 151 us (0.89)
  waiting for transfers between devices: 40.8 us -> 20.6 us
  blocking collectives: 26.7 us -> 30.1 us
    psum x1 -> x0, waiting for transfers between devices: 20.2 us -> none  [on_device(): lax.psum(partial_out, 'tp').astype(jnp.float32)]
    all_gather x0 -> x1, blocking collectives: none -> 2.12 us  [on_device(): jax.lax.all_gather(own_rows, axis_name='tp')]
  transfers between devices with their start and end apart: 3 -> 2, of which waited for: 3 -> 2; matrix products, arithmetic and copies ran while one was open for 1% -> 1% of each run, Pallas kernels for 0% -> 0%
where the time goes in v1:
time: 151 us; the launch traced here: 149 us
  local copies, waits for them, and re-layouts  33.9 us (22%)
  matrix products  33.4 us (22%)
  blocking collectives  30.1 us (20%)
  waiting for transfers between devices  20.6 us (14%)
  between operations  13.6 us (9%)
  other arithmetic  10.9 us (7%)
  starting transfers between devices  6.78 us (4%)
    unnamed x23, local copies, waits for them, and re-layouts  25.3 us
    all_to_all x1, blocking collectives, on_device(): lax.all_to_all(outgoing_half, 'ep', split_axis=0, concat_axis=0, tiled=True)  23.4 us
    all_to_all x1, waiting for transfers between devices, on_device(): lax.all_to_all(share, 'ep', split_axis=0, concat_axis=0, tiled=True)  13.8 us
    dot_general x1, matrix products, expert_work(): jnp.dot(hidden, expert_down, preferred_element_type=jnp.float32)  10.9 us
    all_to_all x1, starting transfers between devices, on_device(): lax.all_to_all(share, 'ep', split_axis=0, concat_axis=0, tiled=True)  6.78 us
    reduce_scatter x1, waiting for transfers between devices, on_device(): lax.psum_scatter(partial_rows, 'tp', scatter_dimension=2, tiled=True)  6.77 us
    dot_general x1, matrix products, expert_work(): jnp.dot(flat_rows, expert_gate, preferred_element_type=jnp.float32)  6.34 us
    dot_general x1, matrix products, attend(): jnp.einsum('skgp,spkd->skgd', weights.reshape(seq_count, kv_count, group_...  5.68 us
  transfers between devices with their start and end apart: 2, of which 2 were waited for; matrix products, arithmetic and copies ran while one was open for 1% of the time, Pallas kernels for 0%

profile of v1, /device:TPU:0, one launch (start us, length us, event | category | flops | bytes accessed | tf_op | source)
XLA Modules:
  0.0 149.4 jit_solution(16886828701489950291)
XLA Ops:
  6.5 0.8 broadcast_add_fusion
  7.3 0.7 iota_compare_fusion.1
  8.1 1.0 fusion.7
  9.1 2.2 %convolution_convert_fusion.3 = bf16[32,512]{1,0:T(8,128)(2,1)S(1)} fusion(bf16[2048,512]{1,0:T(8,128)(2,1)} %param.23, bf16[32,2048]{1,0:T(8,128)(2,1)} %param.17, f32[2048]{0:T(1024)} %param.22, f32[32]{0:T(128)S(1)} %add_rsqrt_fusion.1), kind=kOutput, calls=%fused_computation.9 | convolution fusion | flops 67387392 | bytes 2269312 | tf_op jit(solution)/shard_map/dot_general | solution.py:109
  11.3 0.1 reshape_reshape.3
  11.5 11.9 %copy.45 = bf16[32,1024,128]{1,2,0:T(8,128)(2,1)} copy(bf16[32,1024,128]{2,1,0:T(8,128)(2,1)} %param.19) | data formatting | bytes 16777216 | tf_op args[2]
  23.4 4.6 %convolution_multiply_fusion.1 = f32[32,2,4,1024]{3,2,1,0:T(4,128)S(1)} fusion(bf16[32,2,4,64]{3,2,1,0:T(4,128)(2,1)S(1)} %reshape_reshape.3, bf16[32,1024,2,64]{1,3,2,0:T(8,128)(2,1)} %bitcast.38), kind=kOutput, calls=%fused_computation.6 | convolution fusion | flops 33816576 | bytes 9469952 | tf_op jit(solution)/shard_map/skgd,spkd->skgp/dot_general | solution.py:27
  28.0 1.4 mul.132
  29.4 0.1 iota_compare_fusion
  29.5 1.5 select_reduce_fusion
  31.0 0.2 fusion.15
  31.2 0.1 copy.47
  31.3 1.9 %fusion.25 = (f32[32,8]{1,0:T(8,128)S(1)}, f32[32,8,1024]{2,1,0:T(8,128)S(1)}) fusion(f32[32,8,1024]{2,1,0:T(8,128)} %param.21, f32[32,8,1024]{2,1,0:T(8,128)} %mul.132, f32[32,8]{1,0:T(8,128)S(1)} %copy.47, pred[32,1024]{1,0:T(8,128)(4,1)S(1)} %iota_compare_fusion.1), kind=kLoop, calls=%fused_computation.64 | loop fusion | flops 1048320 | bytes 3180544 | tf_op jit(solution)/shard_map/reduce_max | solution.py:45
  33.3 1.3 convolution_convert_fusion.5
  34.6 0.1 reshape.209
  34.7 0.2 fusion.26
  34.9 0.1 copy.62
  35.0 0.1 copy.49
  35.1 0.3 fusion.3
  35.5 0.1 copy.51
  35.6 1.1 divide_convert_fusion
  36.6 1.2 reshape.188
  37.9 0.1 copy.55
  38.0 1.3 fusion.2
  39.3 0.1 reshape.195
  39.4 11.9 %copy.52 = bf16[32,1024,128]{1,2,0:T(8,128)(2,1)} copy(bf16[32,1024,128]{2,1,0:T(8,128)(2,1)} %param.20) | data formatting | bytes 16777216 | tf_op args[3]
  51.3 5.7 %fusion.1 = bf16[32,2,4,64]{3,2,1,0:T(4,128)(2,1)S(1)} fusion(bf16[32,2,4,1024]{3,2,1,0:T(4,128)(2,1)S(1)} %reshape.188, bf16[32,1024,2,64]{1,3,2,0:T(8,128)(2,1)} %bitcast.39, f32[32,2,64]{2,1,0:T(2,128)S(1)} %reshape.195, f32[32,2,4]{2,1,0:T(2,128)S(1)} %copy.55), kind=kOutput, calls=%fused_computation.8 | convolution fusion | flops 33603584 | bytes 8963072 | tf_op jit(solution)/shard_map/skgp,spkd->skgd/dot_general | solution.py:51
  57.0 0.1 convert_element_type.101
  57.2 0.5 convolution_convert_fusion.2
  57.6 2.1 %all-gather = bf16[64,2048]{1,0:T(8,128)(2,1)S(1)} all-gather(bf16[32,2048]{1,0:T(8,128)(2,1)S(1)} %convolution_convert_fusion.2), channel_id=2, replica_groups=mesh['ep'=16,'tp'=2] {'tp'}, dimensions={0}, use_global_device_ids=true | all-gather | bytes 393216 | tf_op jit(solution)/shard_map/all_gather | solution.py:132
  59.8 0.2 fusion.4
  60.0 0.1 fusion.6
  60.1 0.5 copy-done.3
  60.6 0.1 broadcast_in_dim.61
  60.8 0.1 reshape.191
  60.9 0.1 copy.56
  61.0 0.1 reshape.190
  61.1 0.1 reduce_window_sum.11
  61.2 0.2 select_reduce_fusion.1
  61.4 0.2 convolution_convert_fusion.1
  61.7 0.1 broadcast_in_dim.62
  61.8 0.1 broadcast_in_dim.63
  62.0 23.4 %all_to_all.10 = bf16[16,12,1024]{2,1,0:T(8,128)(2,1)S(1)} all-to-all(bf16[16,12,1024]{2,1,0:T(8,128)(2,1)S(1)} %constant_dynamic-slice_fusion), channel_id=1, replica_groups=mesh['ep'=16,'tp'=2] {'ep'}, dimensions={0} | all-to-all | bytes 786432 | tf_op jit(solution)/shard_map/all_to_all | solution.py:157
  85.4 2.7 %all_gather.14 = bf16[16,12,2048]{2,1,0:T(8,128)(2,1)S(1)} all-gather(bf16[16,12,1024]{2,1,0:T(8,128)(2,1)S(1)} %all_to_all.10), channel_id=1, replica_groups=mesh['ep'=16,'tp'=2] {'tp'}, dimensions={2}, use_global_device_ids=true | all-gather | bytes 1179648 | tf_op jit(solution)/shard_map/all_gather | solution.py:156
  88.1 0.2 reshape.193
  88.3 6.3 %fusion.27 = f32[192,2048]{1,0:T(8,128)} fusion(bf16[192,2048]{1,0:T(8,128)(2,1)S(1)} %reshape.193, bf16[2048,2048]{1,0:T(8,128)(2,1)} %param.31), kind=kOutput, calls=%fused_computation.66 | convolution fusion | flops 1610612736 | bytes 10747904 | tf_op jit(solution)/shard_map/dot_general | solution.py:68
  94.6 10.9 %convolution_convert_fusion = bf16[192,2048]{1,0:T(8,128)(2,1)} fusion(bf16[2048,2048]{1,0:T(8,128)(2,1)} %param.33, bf16[192,2048]{1,0:T(8,128)(2,1)S(1)} %reshape.193, bf16[2048,2048]{1,0:T(8,128)(2,1)} %param.32, f32[192,2048]{1,0:T(8,128)} %fusion.27), kind=kOutput, calls=%fused_computation.2 | convolution fusion | flops 3223977984 | bytes 19922944 | tf_op jit(solution)/shard_map/dot_general | solution.py:71
  105.5 2.1 %convert_element_type.112 = bf16[16,12,2048]{2,1,0:T(8,128)(2,1)} reshape(bf16[192,2048]{1,0:T(8,128)(2,1)} %convolution_convert_fusion) | data formatting | bytes 1572864 | tf_op jit(solution)/shard_map/convert_element_type | solution.py:162
  107.6 0.1 reduce_sum.87
  107.7 6.8 %reduce-scatter.2.cloned.1.call-done = bf16[16,12,1024]{2,1,0:T(8,128)(2,1)} async-done(((bf16[16,12,2048]{2,1,0:T(8,128)(2,1)}), bf16[16,12,1024]{2,1,0:T(8,128)(2,1)}) %reduce-scatter.2.cloned.1.call-update) | async-done | bytes 393232 | tf_op jit(solution)/shard_map/reduce_scatter | solution.py:164
  114.5 6.8 %all-to-all-start.1 = ((bf16[16,12,1024]{2,1,0:T(8,128)(2,1)}), bf16[16,12,1024]{2,1,0:T(8,128)(2,1)S(1)}, u32[]{:S(2)}, u32[]{:S(2)}) async-start(bf16[16,12,1024]{2,1,0:T(8,128)(2,1)} %reduce-scatter.2.cloned.1.call-done), calls=%async_computation.2 | async-start | bytes 1048576 | tf_op jit(solution)/shard_map/all_to_all | solution.py:168
  121.3 0.1 copy.59
  121.4 0.1 mul.152
  121.6 0.7 copy.58
  122.3 0.1 copy.60
  122.4 0.6 pad_clamp_fusion
  123.0 13.8 %all-to-all-done.1 = bf16[16,12,1024]{2,1,0:T(8,128)(2,1)S(1)} async-done(((bf16[16,12,1024]{2,1,0:T(8,128)(2,1)}), bf16[16,12,1024]{2,1,0:T(8,128)(2,1)S(1)}, u32[]{:S(2)}, u32[]{:S(2)}) %all-to-all-start.1) | async-done | bytes 393248 | tf_op jit(solution)/shard_map/all_to_all | solution.py:168
  136.8 0.1 convert_reduce_fusion
  136.9 0.8 gather_fusion
  137.8 0.1 gather.7
  137.9 1.2 multiply_reduce_fusion
  139.1 0.9 add_convert_fusion
  139.9 1.9 %all_gather.15 = bf16[32,2048]{1,0:T(8,128)(2,1)S(1)} all-gather(bf16[32,1024]{1,0:T(8,128)(2,1)S(1)} %add_convert_fusion), channel_id=1, replica_groups=mesh['ep'=16,'tp'=2] {'tp'}, dimensions={1}, use_global_device_ids=true | all-gather | bytes 196608 | tf_op jit(solution)/shard_map/all_gather | solution.py:171
  141.8 0.7 copy.64
  (37 shorter events, 0.6 us)
Async XLA Ops:
  6.5 50.6 %copy-start = (bf16[512,2048]{1,0:T(8,128)(2,1)S(1)}, bf16[512,2048]{1,0:T(8,128)(2,1)}, u32[]{:S(2)}) copy-start(bf16[512,2048]{1,0:T(8,128)(2,1)} %param.27) | copy-start | bytes 6291460
  6.5 108.0 %reduce-scatter.2.cloned.1.call-start = ((), (), s32[]{:S(2)}) async-start(), calls=%async_computation.3 | async-start | bytes 1572864 | tf_op jit(solution)/shard_map/reduce_scatter | solution.py:164
  23.4 7.6 %copy-start.2 = (bf16[32,2048]{1,0:T(8,128)(2,1)S(1)}, bf16[32,2048]{1,0:T(8,128)(2,1)}, u32[]{:S(2)}) copy-start(bf16[32,2048]{1,0:T(8,128)(2,1)} %param.17) | copy-start | bytes 393220
  23.4 7.6 %copy-start.4 = (f32[2048]{0:T(1024)S(1)}, f32[2048]{0:T(1024)}, u32[]{:S(2)}) copy-start(f32[2048]{0:T(1024)} %param.22) | copy-start | bytes 24580
  23.4 7.6 %copy-start.8 = (bf16[2048,8]{0,1:T(8,128)(2,1)S(1)}, bf16[2048,8]{0,1:T(8,128)(2,1)}, u32[]{:S(2)}) copy-start(bf16[2048,8]{0,1:T(8,128)(2,1)} %param.26) | copy-start | bytes 98308
  51.3 8.6 %copy-start.6 = (f32[2048]{0:T(1024)S(1)}, f32[2048]{0:T(1024)}, u32[]{:S(2)}) copy-start(f32[2048]{0:T(1024)} %param.28) | copy-start | bytes 24580
  51.3 9.5 %copy-start.5 = (s32[32,2]{0,1:T(2,128)S(1)}, s32[32,2]{0,1:T(2,128)}, u32[]{:S(2)}) copy-start(s32[32,2]{0,1:T(2,128)} %param.29) | copy-start | bytes 772
  59.9 0.7 copy-start.3
  94.6 27.7 %copy-start.7 = (f32[32,2]{0,1:T(2,128)S(1)}, f32[32,2]{0,1:T(2,128)}, u32[]{:S(2)}) copy-start(f32[32,2]{0,1:T(2,128)} %param.30) | copy-start | bytes 772
  94.6 47.9 %copy-start.1 = (bf16[512,2048]{1,0:T(8,128)(2,1)S(1)}, bf16[512,2048]{1,0:T(8,128)(2,1)}, u32[]{:S(2)}) copy-start(bf16[512,2048]{1,0:T(8,128)(2,1)} %param.27) | copy-start | bytes 6291460
  114.5 22.3 %all-to-all-start.1 = ((bf16[16,12,1024]{2,1,0:T(8,128)(2,1)}), bf16[16,12,1024]{2,1,0:T(8,128)(2,1)S(1)}, u32[]{:S(2)}, u32[]{:S(2)}) async-start(bf16[16,12,1024]{2,1,0:T(8,128)(2,1)} %reduce-scatter.2.cloned.1.call-done), calls=%async_computation.2 | async-start | bytes 1048576 | tf_op jit(solution)/shard_map/all_to_all | solution.py:168
Sparse Core Ops, SparseCore 0:
  107.8 6.7 reduce-scatter.1
